TPU v7x, 32 devices: a whole 2x2x4 slice. The times are simulated.
32 devices in a mesh: grp: 2 (over y), fs: 4 (over z), tp: 4 (over x, core).
Axes of the slice: x: 2, y: 2, z: 4, core: 2. Of those that a mesh axis runs over, the one named last changes fastest.
Arguments:
- tokens: bfloat16 [8192, 2048], P(('grp', 'fs', 'tp')), parts along dimension 0, may hold values from -6 to 6
- norm_gains: float32 [4, 2048], replicated, may hold values from 0.1 to 1.9
- query_weight: bfloat16 [2048, 2048], P('fs', 'tp'), may hold values from -0.125 to 0.125
- key_weight: bfloat16 [2048, 2048], P('fs', 'tp'), may hold values from -0.125 to 0.125
- value_weight: bfloat16 [2048, 4096], P('fs', 'tp'), may hold values from -0.125 to 0.125
- swish_weight: bfloat16 [2048, 4096], P('fs', 'tp'), may hold values from -0.125 to 0.125
- mixer_output: bfloat16 [4096, 2048], P('tp', 'fs'), may hold values from -0.09375 to 0.09375
- gate_weight: bfloat16 [2048, 3072], P('fs', 'tp'), may hold values from -0.125 to 0.125
- up_weight: bfloat16 [2048, 3072], P('fs', 'tp'), may hold values from -0.125 to 0.125
- down_weight: bfloat16 [3072, 2048], P('tp', 'fs'), may hold values from -0.109375 to 0.109375
Outputs:
- layer_output: bfloat16 [8192, 2048], P(('grp', 'fs', 'tp')), parts along dimension 0
There are 2 independent parts, one for each index of `grp`. A program takes and returns all parts, laid end to end along the dimension named above; an argument that names none is the same for every part. Nothing has to cross between parts.
All inputs are finite; a program needn't handle non-finite values.
Results may differ from a plain program's by a relative error of at most 0.02.
Values may be sent and summed in bfloat16 or wider, within the bound.
A program may use at most 128 MiB of HBM per device.

v0:
```python
import jax
import jax.numpy as jnp
from jax import lax
from jax.sharding import PartitionSpec as P

H = 8
QK = 256
BLOCK = 128
norm_epsilon = 1e-06
group_epsilon = 0.01


def rms_scale(matrix, gain):
    return (
        matrix * lax.rsqrt(jnp.mean(matrix * matrix, axis=-1, keepdims=True) + norm_epsilon) * gain
    )


def gather_rows(normed):
    return lax.all_gather(normed, "tp", axis=0, tiled=True)


def add_piece(normed, shard_piece):
    return jnp.dot(normed, shard_piece, preferred_element_type=jnp.float32)


def project_out(active, weight_shard):
    whole_weight = lax.all_gather(weight_shard, "fs", axis=1, tiled=True)
    return lax.psum_scatter(
        jnp.dot(active, whole_weight, preferred_element_type=jnp.float32).astype(jnp.bfloat16),
        "tp",
        scatter_dimension=0,
        tiled=True,
    ).astype(jnp.float32)


def rotate_halves(head_tensors, cosine_table, sine_table):
    half_width = head_tensors.shape[-1] // 2
    lower_half = head_tensors[..., :half_width]
    upper_half = head_tensors[..., half_width:]
    return jnp.concatenate(
        [
            lower_half * cosine_table - upper_half * sine_table,
            lower_half * sine_table + upper_half * cosine_table,
        ],
        axis=-1,
    )


def retention(queries, key_rows, value_rows, log_decay):
    length, head_count, key_width = queries.shape
    value_width = value_rows.shape[-1]
    blocks = length // BLOCK
    query_blocks = queries.reshape(blocks, BLOCK, head_count, key_width)
    key_blocks = key_rows.reshape(blocks, BLOCK, head_count, key_width)
    value_blocks = value_rows.reshape(blocks, BLOCK, head_count, value_width)
    offsets = jnp.arange(BLOCK, dtype=jnp.float32)
    distance = offsets[:, None] - offsets[None, :]
    within = jnp.where(
        distance >= 0, jnp.exp(log_decay[:, None, None] * jnp.maximum(distance, 0.0)), 0.0
    )
    retention_scores = jnp.einsum(
        "cnhd,cmhd->chnm", query_blocks, key_blocks, preferred_element_type=jnp.float32
    )
    local_part = jnp.einsum(
        "chnm,cmhe->cnhe", retention_scores * within[None], value_blocks.astype(jnp.float32)
    )
    key_decay = jnp.exp((BLOCK - 1.0 - offsets)[:, None] * log_decay[None, :])
    query_decay = jnp.exp((offsets + 1.0)[:, None] * log_decay[None, :])
    block_decay = jnp.exp(BLOCK * log_decay)

    def advance(carry_state, inputs):
        query_block, key_block, value_tile = inputs
        carried = (
            jnp.einsum("nhd,hde->nhe", query_block.astype(jnp.float32), carry_state)
            * query_decay[:, :, None]
        )
        decay_weighted = key_block.astype(jnp.float32) * key_decay[:, :, None]
        carry_state = carry_state * block_decay[:, None, None] + jnp.einsum(
            "yui,yua->uia", decay_weighted, value_tile.astype(jnp.float32)
        )
        return (carry_state, carried)

    starting_state = jnp.zeros((head_count, key_width, value_width), jnp.float32)
    _, carried = lax.scan(advance, starting_state, (query_blocks, key_blocks, value_blocks))
    return (local_part + carried).reshape(length, head_count, value_width)


def per_device(
    tokens,
    norm_gains,
    query_weight,
    key_weight,
    value_weight,
    swish_weight,
    mixer_output,
    gate_weight,
    up_weight,
    down_weight,
):
    residual = tokens.astype(jnp.float32)
    normed = gather_rows(rms_scale(residual, norm_gains[0]).astype(jnp.bfloat16))
    pieces = (
        lax.all_gather(query_weight, "fs", axis=0, tiled=True),
        lax.all_gather(key_weight, "fs", axis=0, tiled=True),
        lax.all_gather(value_weight, "fs", axis=0, tiled=True),
        lax.all_gather(swish_weight, "fs", axis=0, tiled=True),
    )
    raw_query, raw_keys, raw_values, raw_swish = tuple(
        (add_piece(normed, shard_piece) for shard_piece in pieces)
    )
    length = normed.shape[0]
    head_count = raw_query.shape[1] // QK
    positions = jnp.arange(length, dtype=jnp.float32)
    frequency = 10000.0 ** (-jnp.linspace(0.0, 1.0, QK // 2, dtype=jnp.float32))
    angles = positions[:, None] * frequency[None, :]
    cosine_table = jnp.cos(angles)[:, None, :]
    sine_table = jnp.sin(angles)[:, None, :]
    queries = rotate_halves(
        raw_query.reshape(length, head_count, QK), cosine_table, sine_table
    ).astype(jnp.bfloat16)
    key_rows = (
        rotate_halves(raw_keys.reshape(length, head_count, QK), cosine_table, sine_table)
        * QK ** (-0.5)
    ).astype(jnp.bfloat16)
    value_rows = raw_values.reshape(length, head_count, -1).astype(jnp.bfloat16)
    head_index = (lax.axis_index("tp") * head_count + jnp.arange(head_count)).astype(jnp.float32)
    log_decay = -(4.0 / BLOCK) * (BLOCK / (32.0 * length)) ** (head_index / (H - 1))
    retained = retention(queries, key_rows, value_rows, log_decay)
    centred = retained - jnp.mean(retained, axis=-1, keepdims=True)
    normalized = centred * lax.rsqrt(
        jnp.mean(centred * centred, axis=-1, keepdims=True) + group_epsilon
    )
    gated_rows = (jax.nn.silu(raw_swish) * normalized.reshape(length, -1)).astype(jnp.bfloat16)
    mixer_total = project_out(gated_rows, mixer_output)
    after_mixer = residual + rms_scale(mixer_total, norm_gains[1])
    widened = gather_rows(rms_scale(after_mixer, norm_gains[2]).astype(jnp.bfloat16))
    pieces = (
        lax.all_gather(gate_weight, "fs", axis=0, tiled=True),
        lax.all_gather(up_weight, "fs", axis=0, tiled=True),
    )
    gate_sum = add_piece(widened, pieces[0])
    up_sum = add_piece(widened, pieces[1])
    hidden = (jax.nn.silu(gate_sum) * up_sum).astype(jnp.bfloat16)
    channel = project_out(hidden, down_weight)
    return (after_mixer + rms_scale(channel, norm_gains[3])).astype(jnp.bfloat16)


def solution(mesh):
    placed = (
        P(("grp", "fs", "tp"), None),
        P(),
        P("fs", "tp"),
        P("fs", "tp"),
        P("fs", "tp"),
        P("fs", "tp"),
        P("tp", "fs"),
        P("fs", "tp"),
        P("fs", "tp"),
        P("tp", "fs"),
    )
    return jax.shard_map(
        per_device,
        mesh=mesh,
        in_specs=placed,
        out_specs=P(("grp", "fs", "tp"), None),
        check_vma=False,
    )
```

profile of v0, /device:TPU:0, one launch (start us, length us, event | category | flops | bytes accessed | tf_op | source)
XLA Modules:
  0.0 738.8 jit_solution(8517248313428038904)
XLA Ops:
  7.3 1.5 fusion.23
  9.8 2.5 fusion.25
  15.0 2.8 fusion.31
  18.0 39.4 %all-gather.17.cloned.1.call-done = bf16[2048,512]{1,0:T(8,128)(2,1)} async-done(((bf16[512,512]{1,0:T(8,128)(2,1)}), bf16[2048,512]{1,0:T(8,128)(2,1)}) %all-gather.17.cloned.1.call-update) | async-done | bytes 2097168 | tf_op jit(solution)/shard_map/all_gather | solution.py:104
  57.3 34.8 %all-gather.11.cloned.1.call-done = bf16[1024,2048]{1,0:T(8,128)(2,1)} async-done(((bf16[256,2048]{1,0:T(8,128)(2,1)}), bf16[1024,2048]{1,0:T(8,128)(2,1)}) %all-gather.11.cloned.1.call-update) | async-done | bytes 4194320 | tf_op jit(solution)/shard_map/all_gather | solution.py:20
  92.2 5.2 fusion.48
  97.6 1.3 copy.49
  98.9 1.3 copy.50
  100.2 39.2 %all-gather.19.cloned.1.call-done = bf16[2048,512]{1,0:T(8,128)(2,1)} async-done(((bf16[512,512]{1,0:T(8,128)(2,1)}), bf16[2048,512]{1,0:T(8,128)(2,1)}) %all-gather.19.cloned.1.call-update) | async-done | bytes 2097168 | tf_op jit(solution)/shard_map/all_gather | solution.py:105
  139.4 5.2 fusion.49
  144.8 1.3 copy.51
  146.1 1.3 copy.52
  147.5 4.4 subtract_convert_fusion
  154.0 66.5 %all-gather.15.cloned.1.call-done = bf16[2048,1024]{1,0:T(8,128)(2,1)} async-done(((bf16[512,1024]{1,0:T(8,128)(2,1)}), bf16[2048,1024]{1,0:T(8,128)(2,1)}) %all-gather.15.cloned.1.call-update) | async-done | bytes 4194320 | tf_op jit(solution)/shard_map/all_gather | solution.py:106
  220.4 9.3 %convolution_convert_fusion.2 = bf16[1024,1024]{1,0:T(8,128)(2,1)} fusion(bf16[1024,2048]{1,0:T(8,128)(2,1)} %all-gather.11.cloned.1.call-done, bf16[2048,1024]{1,0:T(8,128)(2,1)} %all-gather.15.cloned.1.call-done), kind=kOutput, calls=%fused_computation.53 | convolution fusion | flops 4296015872 | bytes 10485760 | tf_op jit(solution)/shard_map/dot_general | solution.py:24
  229.8 4.5 convert_element_type.66
  234.3 1.4 fusion.26
  235.8 31.7 %while.15 = (s32[]{:T(128)}, f32[2,256,512]{2,1,0:T(8,128)S(1)}, f32[8,128,2,512]{1,3,2,0:T(8,128)}, bf16[8,128,2,256]{3,1,2,0:T(8,128)(2,1)S(1)}, bf16[8,128,2,...) while((s32[]{:T(128)}, f32[2,256,512]{2,1,0:T(8,128)S(1)}, ...), condition=%wide.region_2.3_spmd.clone.clone.clone, body=%wide.region_1.2_spmd.clone.clone.clone.sunk | while | flops 135528960 | bytes 7346340 | solution.py:85
  235.8 1.1 fusion.71
  239.8 1.1 fusion.71
  241.0 1.1 constant_dynamic-slice_fusion.4
  247.8 1.1 fusion.71
  251.7 1.1 fusion.71
  263.6 1.1 fusion.71
  267.5 6.3 fusion.43
  273.8 7.2 copy.40
  281.0 2.6 multiply_reduce_fusion
  283.9 1.4 mul.345
  285.3 3.0 copy.61
  288.5 1.4 sub.74
  289.9 3.1 copy.60
  292.9 3.0 copy.59
  295.9 5.2 all-gather.13.cloned.1.call-done
  301.1 80.7 %all-gather.21.cloned.1.call-done = bf16[1024,2048]{1,0:T(8,128)(2,1)} async-done(((bf16[1024,512]{1,0:T(8,128)(2,1)}), bf16[1024,2048]{1,0:T(8,128)(2,1)}) %all-gather.21.cloned.1.call-update) | async-done | bytes 4194320 | tf_op jit(solution)/shard_map/all_gather | solution.py:28
  381.8 17.5 %convolution_convert_fusion.1 = bf16[1024,2048]{1,0:T(8,128)(2,1)} fusion(bf16[1024,2048]{1,0:T(8,128)(2,1)} %all-gather.21.cloned.1.call-done, f32[1024,1024]{1,0:T(8,128)} %bitcast.75, f32[1024,1024]{1,0:T(8,128)} %bitcast.77, f32[1024,1024]{1,0:T(8,128)} %bitcast.76, bf16[1024,2048]{1,0:T(8,128)(2,1)} %all-gather.11.cloned.1.call-done, ...), kind=kOutput, calls=%fused_computation.28 | convolution fusion | flops 8600420352 | bytes 29360128 | tf_op jit(solution)/shard_map/dot_general | solution.py:30
  400.1 42.4 %reduce-scatter.3.cloned.1.call-done = bf16[256,2048]{1,0:T(8,128)(2,1)} async-done(((bf16[1024,2048]{1,0:T(8,128)(2,1)}), bf16[256,2048]{1,0:T(8,128)(2,1)}) %reduce-scatter.3.cloned.1.call-update) | async-done | bytes 1048592 | tf_op jit(solution)/shard_map/reduce_scatter | solution.py:29
  442.6 1.6 fusion.17
  444.2 1.8 multiply_reduce_fusion.1
  446.0 1.6 multiply_convert_fusion.3
  449.2 58.4 %all-gather.25.cloned.1.call-done = bf16[2048,768]{1,0:T(8,128)(2,1)} async-done(((bf16[512,768]{1,0:T(8,128)(2,1)}), bf16[2048,768]{1,0:T(8,128)(2,1)}) %all-gather.25.cloned.1.call-update) | async-done | bytes 3145744 | tf_op jit(solution)/shard_map/all_gather | solution.py:139
  507.6 34.7 %all-gather.23.cloned.1.call-done = bf16[1024,2048]{1,0:T(8,128)(2,1)} async-done(((bf16[256,2048]{1,0:T(8,128)(2,1)}), bf16[1024,2048]{1,0:T(8,128)(2,1)}) %all-gather.23.cloned.1.call-update) | async-done | bytes 4194320 | tf_op jit(solution)/shard_map/all_gather | solution.py:20
  542.3 8.2 %fusion.50 = f32[1024,768]{1,0:T(8,128)} fusion(bf16[1024,2048]{1,0:T(8,128)(2,1)} %all-gather.23.cloned.1.call-done, bf16[2048,768]{1,0:T(8,128)(2,1)} %all-gather.25.cloned.1.call-done), kind=kOutput, calls=%fused_computation.91 | convolution fusion | flops 3221225472 | bytes 10485760 | tf_op jit(solution)/shard_map/dot_general | solution.py:24
  550.5 56.7 %all-gather.27.cloned.1.call-done = bf16[2048,768]{1,0:T(8,128)(2,1)} async-done(((bf16[512,768]{1,0:T(8,128)(2,1)}), bf16[2048,768]{1,0:T(8,128)(2,1)}) %all-gather.27.cloned.1.call-update) | async-done | bytes 3145744 | tf_op jit(solution)/shard_map/all_gather | solution.py:140
  607.2 63.7 %all-gather.29.cloned.1.call-done = bf16[768,2048]{1,0:T(8,128)(2,1)} async-done(((bf16[768,512]{1,0:T(8,128)(2,1)}), bf16[768,2048]{1,0:T(8,128)(2,1)}) %all-gather.29.cloned.1.call-update) | async-done | bytes 3145744 | tf_op jit(solution)/shard_map/all_gather | solution.py:28
  670.9 13.2 %convolution_convert_fusion = bf16[1024,2048]{1,0:T(8,128)(2,1)} fusion(bf16[768,2048]{1,0:T(8,128)(2,1)} %all-gather.29.cloned.1.call-done, f32[1024,768]{1,0:T(8,128)} %fusion.50, bf16[1024,2048]{1,0:T(8,128)(2,1)} %all-gather.23.cloned.1.call-done, bf16[2048,768]{1,0:T(8,128)(2,1)} %all-gather.27.cloned.1.call-done), kind=kOutput, calls=%fused_computation.27 | convolution fusion | flops 6449266688 | bytes 17825792 | tf_op jit(solution)/shard_map/dot_general | solution.py:30
  684.1 43.4 %reduce-scatter.5.cloned.1.call-done = bf16[256,2048]{1,0:T(8,128)(2,1)} async-done(((bf16[1024,2048]{1,0:T(8,128)(2,1)}), bf16[256,2048]{1,0:T(8,128)(2,1)}) %reduce-scatter.5.cloned.1.call-update) | async-done | bytes 1048592 | tf_op jit(solution)/shard_map/reduce_scatter | solution.py:29
  727.5 1.5 fusion.19
  729.0 2.9 fusion.22
  (122 shorter events, 34.2 us)
Async XLA Ops:
  6.5 50.8 %all-gather.17.cloned.1.call-start = ((), (), s32[]{:S(2)}) async-start(), calls=%async_computation.5 | async-start | bytes 2621440 | tf_op jit(solution)/shard_map/all_gather | solution.py:104
  7.3 84.9 %all-gather.11.cloned.1.call-start = ((), (), s32[]{:S(2)}) async-start(), calls=%async_computation.2 | async-start | bytes 5242880 | tf_op jit(solution)/shard_map/all_gather | solution.py:20
  12.3 127.1 %all-gather.19.cloned.1.call-start = ((), (), s32[]{:S(2)}) async-start(), calls=%async_computation.6 | async-start | bytes 2621440 | tf_op jit(solution)/shard_map/all_gather | solution.py:105
  13.0 207.4 %all-gather.15.cloned.1.call-start = ((), (), s32[]{:S(2)}) async-start(), calls=%async_computation.4 | async-start | bytes 5242880 | tf_op jit(solution)/shard_map/all_gather | solution.py:106
  13.6 287.5 %all-gather.13.cloned.1.call-start = ((), (), s32[]{:S(2)}) async-start(), calls=%async_computation.3 | async-start | bytes 5242880 | tf_op jit(solution)/shard_map/all_gather | solution.py:107
  14.2 367.6 %all-gather.21.cloned.1.call-start = ((), (), s32[]{:S(2)}) async-start(), calls=%async_computation.7 | async-start | bytes 5242880 | tf_op jit(solution)/shard_map/all_gather | solution.py:28
  14.8 427.8 %reduce-scatter.3.cloned.1.call-start = ((), (), s32[]{:S(2)}) async-start(), calls=%async_computation.8 | async-start | bytes 5242880 | tf_op jit(solution)/shard_map/reduce_scatter | solution.py:29
  151.8 0.8 copy-start.3
  151.8 1.0 copy-start.4
  289.9 3.1 copy-start.1
  399.3 44.9 %copy-start = (bf16[256,2048]{1,0:T(8,128)(2,1)S(1)}, bf16[256,2048]{1,0:T(8,128)(2,1)}, u32[]{:S(2)}) copy-start(bf16[256,2048]{1,0:T(8,128)(2,1)} %param.12) | copy-start | bytes 3145732
  399.3 108.3 %all-gather.25.cloned.1.call-start = ((), (), s32[]{:S(2)}) async-start(), calls=%async_computation.10 | async-start | bytes 3932160 | tf_op jit(solution)/shard_map/all_gather | solution.py:139
  400.1 142.2 %all-gather.23.cloned.1.call-start = ((), (), s32[]{:S(2)}) async-start(), calls=%async_computation.9 | async-start | bytes 5242880 | tf_op jit(solution)/shard_map/all_gather | solution.py:20
  442.5 3.5 copy-start.2
  447.6 159.5 %all-gather.27.cloned.1.call-start = ((), (), s32[]{:S(2)}) async-start(), calls=%async_computation.11 | async-start | bytes 3932160 | tf_op jit(solution)/shard_map/all_gather | solution.py:140
  448.2 222.7 %all-gather.29.cloned.1.call-start = ((), (), s32[]{:S(2)}) async-start(), calls=%async_computation.12 | async-start | bytes 3932160 | tf_op jit(solution)/shard_map/all_gather | solution.py:28
  449.0 278.5 %reduce-scatter.5.cloned.1.call-start = ((), (), s32[]{:S(2)}) async-start(), calls=%async_computation.13 | async-start | bytes 5242880 | tf_op jit(solution)/shard_map/reduce_scatter | solution.py:29
Sparse Core Ops, SparseCore 0:
  8.9 48.3 all-gather.16
  58.9 33.2 all-gather.10
  93.8 45.6 all-gather.18
  140.9 79.5 all-gather.14
  221.9 79.2 all-gather.12
  302.5 79.2 all-gather.20
  399.4 43.0 reduce-scatter.2
  444.1 63.4 all-gather.24
  509.2 33.0 all-gather.22
  543.7 63.4 all-gather.26
  608.8 62.0 all-gather.28
  684.2 43.2 reduce-scatter.4
where the time goes:
time: 740 us; the launch traced here: 739 us
  waiting for transfers between devices  570 us (77%)
  matrix products  77.2 us (10%)
  local copies, waits for them, and re-layouts  51 us (7%)
  other arithmetic  25.9 us (4%)
  between operations  13.7 us (2%)
    all_gather x2, waiting for transfers between devices, project_out(): whole_weight = lax.all_gather(weight_shard, 'fs', axis=1, tiled=True)  144 us
    reduce_scatter x2, waiting for transfers between devices, project_out(): lax.psum_scatter(jnp.dot(active, whole_weight, preferred_element_type=jnp...  85.8 us
    all_gather x2, waiting for transfers between devices, gather_rows(): return lax.all_gather(normed, 'tp', axis=0, tiled=True)  69.5 us
    all_gather x1, waiting for transfers between devices, per_device(): lax.all_gather(value_weight, 'fs', axis=0, tiled=True)  66.5 us
    all_gather x1, waiting for transfers between devices, per_device(): lax.all_gather(gate_weight, 'fs', axis=0, tiled=True)  58.4 us
    all_gather x1, waiting for transfers between devices, per_device(): lax.all_gather(up_weight, 'fs', axis=0, tiled=True)  56.7 us
    all_gather x1, waiting for transfers between devices, per_device(): lax.all_gather(query_weight, 'fs', axis=0, tiled=True)  39.4 us
    all_gather x1, waiting for transfers between devices, per_device(): lax.all_gather(key_weight, 'fs', axis=0, tiled=True)  39.2 us
  transfers between devices with their start and end apart: 12, of which 12 were waited for; matrix products, arithmetic and copies ran while one was open for 16% of the time, Pallas kernels for 0%

commit v1 on v0

--- a/solution.py
+++ b/solution.py
@@ -25,7 +25,14 @@
 
 
 def project_out(active, weight_shard):
-    whole_weight = lax.all_gather(weight_shard, "fs", axis=1, tiled=True)
+    count = lax.axis_size("fs")
+    right = [(i, (i + 1) % count) for i in range(count)]
+    parts = [weight_shard]
+    for hop in range(1, count):
+        parts = [lax.ppermute(parts[0], "fs", right), *parts]
+    full = jnp.concatenate(parts, axis=1)
+    shift = (lax.axis_index("fs") + 1) * parts[-1].shape[1]
+    whole_weight = jnp.roll(full, shift, axis=1)
     return lax.psum_scatter(
         jnp.dot(active, whole_weight, preferred_element_type=jnp.float32).astype(jnp.bfloat16),
         "tp",

time: 740 us -> 646 us (0.87)
  waiting for transfers between devices: 570 us -> 418 us
  starting transfers between devices: 0.65 us -> 34.2 us
  local copies, waits for them, and re-layouts: 51 us -> 73.3 us
    ppermute x0 -> x6, waiting for transfers between devices: none -> 183 us  [project_out(): parts = [lax.ppermute(parts[0], 'fs', right), *parts]]
    all_gather x2 -> x0, waiting for transfers between devices: 144 us -> none  [project_out(): whole_weight = lax.all_gather(weight_shard, 'fs', axis=1, tiled=True)]
    all_gather x2, waiting for transfers between devices: 69.5 us -> 7.48 us  [gather_rows(): return lax.all_gather(normed, 'tp', axis=0, tiled=True)]
    all_gather x1, waiting for transfers between devices: 58.4 us -> 0.01 us  [per_device(): lax.all_gather(gate_weight, 'fs', axis=0, tiled=True)]
    all_gather x1, waiting for transfers between devices: 39.4 us -> 0.01 us  [per_device(): lax.all_gather(query_weight, 'fs', axis=0, tiled=True)]
    ppermute x0 -> x6, starting transfers between devices: none -> 33.8 us  [project_out(): parts = [lax.ppermute(parts[0], 'fs', right), *parts]]
    all_gather x1, waiting for transfers between devices: 39.2 us -> 10.6 us  [per_device(): lax.all_gather(key_weight, 'fs', axis=0, tiled=True)]
    unnamed x17 -> x35, local copies, waits for them, and re-layouts: 15.1 us -> 35.2 us
  transfers between devices with their start and end apart: 12 -> 16, of which waited for: 12 -> 13; matrix products, arithmetic and copies ran while one was open for 16% -> 22% of each run, Pallas kernels for 0% -> 0%
where the time goes in v1:
time: 646 us; the launch traced here: 644 us
  waiting for transfers between devices  418 us (65%)
  matrix products  77.1 us (12%)
  local copies, waits for them, and re-layouts  73.3 us (11%)
  starting transfers between devices  34.2 us (5%)
  other arithmetic  27 us (4%)
  between operations  13.8 us (2%)
    ppermute x6, waiting for transfers between devices, project_out(): parts = [lax.ppermute(parts[0], 'fs', right), *parts]  183 us
    reduce_scatter x2, waiting for transfers between devices, project_out(): lax.psum_scatter(jnp.dot(active, whole_weight, preferred_element_type=jnp...  85.8 us
    all_gather x1, waiting for transfers between devices, per_device(): lax.all_gather(value_weight, 'fs', axis=0, tiled=True)  66.2 us
    all_gather x1, waiting for transfers between devices, per_device(): lax.all_gather(up_weight, 'fs', axis=0, tiled=True)  56.9 us
    unnamed x35, local copies, waits for them, and re-layouts  35.2 us
    ppermute x6, starting transfers between devices, project_out(): parts = [lax.ppermute(parts[0], 'fs', right), *parts]  33.8 us
    dot_general x2, matrix products, project_out(): jnp.dot(active, whole_weight, preferred_element_type=jnp.float32)  30.6 us
    dot_general x4, matrix products, add_piece(): return jnp.dot(normed, shard_piece, preferred_element_type=jnp.float32)  28 us
  transfers between devices with their start and end apart: 16, of which 13 were waited for; matrix products, arithmetic and copies ran while one was open for 22% of the time, Pallas kernels for 0%

profile of v1, /device:TPU:0, one launch (start us, length us, event | category | flops | bytes accessed | tf_op | source)
XLA Modules:
  0.0 644.3 jit_solution(6298005504714603084)
XLA Ops:
  7.3 1.5 fusion.29
  9.8 2.5 fusion.31
  13.7 3.1 collective-permute-start
  16.8 44.1 %collective-permute-done = bf16[1024,512]{1,0:T(8,128)(2,1)S(1)} collective-permute-done((bf16[1024,512]{1,0:T(8,128)(2,1)S(1)}, bf16[1024,512]{1,0:T(8,128)(2,1)S(1)}, u32[]{:S(2)}, u32[]{:S(2)}) %collective-permute-start) | collective-permute-done | bytes 1048608 | tf_op jit(solution)/shard_map/ppermute | solution.py:32
  60.9 13.6 %collective-permute-start.1 = (bf16[1024,512]{1,0:T(8,128)(2,1)S(1)}, bf16[1024,512]{1,0:T(8,128)(2,1)}, u32[]{:S(2)}, u32[]{:S(2)}) collective-permute-start(bf16[1024,512]{1,0:T(8,128)(2,1)S(1)} %collective-permute-done), channel_id=1, source_target_pairs={{0,4},{4,8},{8,12},{12,0},{1,5},{5,9},{9,13},{13,1},{2,6},{6,10},{... | collective-permute-start | bytes 3145736 | tf_op jit(solution)/shard_map/ppermute | solution.py:32
  74.6 25.3 %collective-permute-done.1 = bf16[1024,512]{1,0:T(8,128)(2,1)} collective-permute-done((bf16[1024,512]{1,0:T(8,128)(2,1)S(1)}, bf16[1024,512]{1,0:T(8,128)(2,1)}, u32[]{:S(2)}, u32[]{:S(2)}) %collective-permute-start.1) | collective-permute-done | bytes 1048608 | tf_op jit(solution)/shard_map/ppermute | solution.py:32
  100.1 2.8 fusion.37
  103.0 24.2 %collective-permute-done.2 = bf16[1024,512]{1,0:T(8,128)(2,1)} collective-permute-done((bf16[1024,512]{1,0:T(8,128)(2,1)}, bf16[1024,512]{1,0:T(8,128)(2,1)}, u32[]{:S(2)}, u32[]{:S(2)}) %collective-permute-start.2) | collective-permute-done | bytes 1048608 | tf_op jit(solution)/shard_map/ppermute | solution.py:32
  127.1 2.4 constant_dynamic-update-slice_fusion.8
  129.5 2.3 constant_dynamic-update-slice_fusion.7
  134.1 2.4 constant_dynamic-update-slice_fusion.4
  136.5 2.4 constant_dynamic-update-slice_fusion.3
  141.1 5.3 fusion.56
  146.5 1.4 copy.49
  149.2 10.6 %all-gather.17.cloned.1.call-done = bf16[2048,512]{1,0:T(8,128)(2,1)} async-done(((bf16[512,512]{1,0:T(8,128)(2,1)}), bf16[2048,512]{1,0:T(8,128)(2,1)}) %all-gather.17.cloned.1.call-update) | async-done | bytes 2097168 | tf_op jit(solution)/shard_map/all_gather | solution.py:112
  159.8 5.2 fusion.57
  167.9 4.4 subtract_convert_fusion
  174.3 66.2 %all-gather.13.cloned.1.call-done = bf16[2048,1024]{1,0:T(8,128)(2,1)} async-done(((bf16[512,1024]{1,0:T(8,128)(2,1)}), bf16[2048,1024]{1,0:T(8,128)(2,1)}) %all-gather.13.cloned.1.call-update) | async-done | bytes 4194320 | tf_op jit(solution)/shard_map/all_gather | solution.py:113
  240.5 9.3 %convolution_convert_fusion.1 = bf16[1024,1024]{1,0:T(8,128)(2,1)} fusion(bf16[1024,2048]{1,0:T(8,128)(2,1)} %all-gather.9.cloned.1.call-done, bf16[2048,1024]{1,0:T(8,128)(2,1)} %all-gather.13.cloned.1.call-done), kind=kOutput, calls=%fused_computation.56 | convolution fusion | flops 4296015872 | bytes 10485760 | tf_op jit(solution)/shard_map/dot_general | solution.py:24
  249.8 4.6 convert_element_type.66
  254.5 1.4 fusion.32
  255.9 31.8 %while.15 = (s32[]{:T(128)}, f32[2,256,512]{2,1,0:T(8,128)S(1)}, f32[8,128,2,512]{1,3,2,0:T(8,128)}, bf16[8,128,2,256]{3,1,2,0:T(8,128)(2,1)S(1)}, bf16[8,128,2,...) while((s32[]{:T(128)}, f32[2,256,512]{2,1,0:T(8,128)S(1)}, ...), condition=%wide.region_2.3_spmd.clone.clone.clone, body=%wide.region_1.2_spmd.clone.clone.clone.sunk | while | flops 135528960 | bytes 7346340 | solution.py:92
  287.7 6.4 fusion.51
  294.1 7.2 %copy.40 = f32[8,128,2,512]{3,2,1,0:T(2,128)} copy(f32[8,128,2,512]{1,3,2,0:T(8,128)} %get-tuple-element.223) | data formatting | bytes 8388608 | tf_op jit(solution)/shard_map/add | solution.py:93
  301.4 2.6 multiply_reduce_fusion
  304.3 1.4 mul.349
  305.7 3.0 copy.61
  308.9 1.4 sub.80
  310.3 3.0 copy.60
  313.3 3.0 copy.59
  316.3 4.9 all-gather.11.cloned.1.call-done
  321.2 17.5 %fusion.19 = bf16[1024,2048]{1,0:T(8,128)(2,1)} fusion(bf16[1024,4096]{1,0:T(8,128)(2,1)} %constant_dynamic-update-slice_fusion.1, s32[]{:T(128)S(6)} %select_n.29, f32[1024,1024]{1,0:T(8,128)} %bitcast.73, f32[1024,1024]{1,0:T(8,128)} %bitcast.75, f32[1024,1024]{1,0:T(8,128)} %bitcast.74, bf16[1024,2048]{1,0:T(8,128)(2,1)} %all-gather.9.cloned.1.call-done, ...), kind=kOutput, calls=%fused_computation.29 | convolution fusion | flops 8600420352 | bytes 29360132 | tf_op jit(solution)/shard_map/dot_general | solution.py:37
  339.5 42.4 %reduce-scatter.3.cloned.1.call-done = bf16[256,2048]{1,0:T(8,128)(2,1)} async-done(((bf16[1024,2048]{1,0:T(8,128)(2,1)}), bf16[256,2048]{1,0:T(8,128)(2,1)}) %reduce-scatter.3.cloned.1.call-update) | async-done | bytes 1048592 | tf_op jit(solution)/shard_map/reduce_scatter | solution.py:36
  381.9 1.5 fusion.23
  383.5 1.8 multiply_reduce_fusion.1
  385.3 2.8 multiply_convert_fusion.3
  388.9 1.8 collective-permute-start.3
  390.7 34.9 %collective-permute-done.3 = bf16[768,512]{1,0:T(8,128)(2,1)S(1)} collective-permute-done((bf16[768,512]{1,0:T(8,128)(2,1)S(1)}, bf16[768,512]{1,0:T(8,128)(2,1)S(1)}, u32[]{:S(2)}, u32[]{:S(2)}) %collective-permute-start.3) | collective-permute-done | bytes 786464 | tf_op jit(solution)/shard_map/ppermute | solution.py:32
  425.5 15.4 %collective-permute-start.4 = (bf16[768,512]{1,0:T(8,128)(2,1)S(1)}, bf16[768,512]{1,0:T(8,128)(2,1)S(1)}, u32[]{:S(2)}, u32[]{:S(2)}) collective-permute-start(bf16[768,512]{1,0:T(8,128)(2,1)S(1)} %collective-permute-done.3), channel_id=1, source_target_pairs={{0,4},{4,8},{8,12},{12,0},{1,5},{5,9},{9,13},{13,1},{2,6},{6,10},{... | collective-permute-start | bytes 2359304 | tf_op jit(solution)/shard_map/ppermute | solution.py:32
  441.0 36.7 %collective-permute-done.4 = bf16[768,512]{1,0:T(8,128)(2,1)S(1)} collective-permute-done((bf16[768,512]{1,0:T(8,128)(2,1)S(1)}, bf16[768,512]{1,0:T(8,128)(2,1)S(1)}, u32[]{:S(2)}, u32[]{:S(2)}) %collective-permute-start.4) | collective-permute-done | bytes 786464 | tf_op jit(solution)/shard_map/ppermute | solution.py:32
  477.6 18.0 %collective-permute-done.5 = bf16[768,512]{1,0:T(8,128)(2,1)S(1)} collective-permute-done((bf16[768,512]{1,0:T(8,128)(2,1)S(1)}, bf16[768,512]{1,0:T(8,128)(2,1)S(1)}, u32[]{:S(2)}, u32[]{:S(2)}) %collective-permute-start.5) | collective-permute-done | bytes 786464 | tf_op jit(solution)/shard_map/ppermute | solution.py:32
  503.9 7.5 %all-gather.19.cloned.1.call-done = bf16[1024,2048]{1,0:T(8,128)(2,1)} async-done(((bf16[256,2048]{1,0:T(8,128)(2,1)}), bf16[1024,2048]{1,0:T(8,128)(2,1)}) %all-gather.19.cloned.1.call-update) | async-done | bytes 4194320 | tf_op jit(solution)/shard_map/all_gather | solution.py:20
  511.4 8.2 %fusion.58 = f32[1024,768]{1,0:T(8,128)} fusion(bf16[1024,2048]{1,0:T(8,128)(2,1)} %all-gather.19.cloned.1.call-done, bf16[2048,768]{1,0:T(8,128)(2,1)} %all-gather.21.cloned.1.call-done), kind=kOutput, calls=%fused_computation.112 | convolution fusion | flops 3221225472 | bytes 10485760 | tf_op jit(solution)/shard_map/dot_general | solution.py:24
  519.6 56.9 %all-gather.23.cloned.1.call-done = bf16[2048,768]{1,0:T(8,128)(2,1)} async-done(((bf16[512,768]{1,0:T(8,128)(2,1)}), bf16[2048,768]{1,0:T(8,128)(2,1)}) %all-gather.23.cloned.1.call-update) | async-done | bytes 3145744 | tf_op jit(solution)/shard_map/all_gather | solution.py:147
  576.4 13.1 %convolution_convert_fusion = bf16[1024,2048]{1,0:T(8,128)(2,1)} fusion(bf16[768,4096]{1,0:T(8,128)(2,1)} %constant_dynamic-update-slice_fusion.9, s32[]{:T(128)S(6)} %select_n.29, f32[1024,768]{1,0:T(8,128)} %fusion.58, bf16[1024,2048]{1,0:T(8,128)(2,1)} %all-gather.19.cloned.1.call-done, bf16[2048,768]{1,0:T(8,128)(2,1)} %all-gather.23.cloned.1.call-done), kind=kOutput, calls=%fused_computation.30 | convolution fusion | flops 6449266688 | bytes 17825796 | tf_op jit(solution)/shard_map/dot_general | solution.py:37
  589.6 43.4 %reduce-scatter.5.cloned.1.call-done = bf16[256,2048]{1,0:T(8,128)(2,1)} async-done(((bf16[1024,2048]{1,0:T(8,128)(2,1)}), bf16[256,2048]{1,0:T(8,128)(2,1)}) %reduce-scatter.5.cloned.1.call-update) | async-done | bytes 1048592 | tf_op jit(solution)/shard_map/reduce_scatter | solution.py:36
  633.0 1.5 fusion.25
  634.5 2.9 fusion.28
  (148 shorter events, 55.8 us)
Async XLA Ops:
  6.5 7.1 %copy-start.5 = (bf16[1024,512]{1,0:T(8,128)(2,1)S(1)}, bf16[1024,512]{1,0:T(8,128)(2,1)}, u32[]{:S(2)}) copy-start(bf16[1024,512]{1,0:T(8,128)(2,1)} %param.18) | copy-start | bytes 3145732
  6.5 134.6 %all-gather.15.cloned.1.call-start = ((), (), s32[]{:S(2)}) async-start(), calls=%async_computation.5 | async-start | bytes 2621440 | tf_op jit(solution)/shard_map/all_gather | solution.py:111
  7.3 133.8 %all-gather.9.cloned.1.call-start = ((), (), s32[]{:S(2)}) async-start(), calls=%async_computation.2 | async-start | bytes 5242880 | tf_op jit(solution)/shard_map/all_gather | solution.py:20
  12.3 147.5 %all-gather.17.cloned.1.call-start = ((), (), s32[]{:S(2)}) async-start(), calls=%async_computation.6 | async-start | bytes 2621440 | tf_op jit(solution)/shard_map/all_gather | solution.py:112
  13.0 227.5 %all-gather.13.cloned.1.call-start = ((), (), s32[]{:S(2)}) async-start(), calls=%async_computation.4 | async-start | bytes 5242880 | tf_op jit(solution)/shard_map/all_gather | solution.py:113
  13.6 307.6 %all-gather.11.cloned.1.call-start = ((), (), s32[]{:S(2)}) async-start(), calls=%async_computation.3 | async-start | bytes 5242880 | tf_op jit(solution)/shard_map/all_gather | solution.py:114
  13.7 47.3 %collective-permute-start = (bf16[1024,512]{1,0:T(8,128)(2,1)S(1)}, bf16[1024,512]{1,0:T(8,128)(2,1)S(1)}, u32[]{:S(2)}, u32[]{:S(2)}) collective-permute-start(bf16[1024,512]{1,0:T(8,128)(2,1)S(1)} %copy-done.5), channel_id=1, source_target_pairs={{0,4},{4,8},{8,12},{12,0},{1,5},{5,9},{9,13},{13,1},{2,6},{6,10},{... | collective-permute-start | bytes 3145736 | tf_op jit(solution)/shard_map/ppermute | solution.py:32
  60.9 38.9 %collective-permute-start.1 = (bf16[1024,512]{1,0:T(8,128)(2,1)S(1)}, bf16[1024,512]{1,0:T(8,128)(2,1)}, u32[]{:S(2)}, u32[]{:S(2)}) collective-permute-start(bf16[1024,512]{1,0:T(8,128)(2,1)S(1)} %collective-permute-done), channel_id=1, source_target_pairs={{0,4},{4,8},{8,12},{12,0},{1,5},{5,9},{9,13},{13,1},{2,6},{6,10},{... | collective-permute-start | bytes 3145736 | tf_op jit(solution)/shard_map/ppermute | solution.py:32
  74.5 307.4 %reduce-scatter.3.cloned.1.call-start = ((), (), s32[]{:S(2)}) async-start(), calls=%async_computation.7 | async-start | bytes 5242880 | tf_op jit(solution)/shard_map/reduce_scatter | solution.py:36
  99.8 27.3 %collective-permute-start.2 = (bf16[1024,512]{1,0:T(8,128)(2,1)}, bf16[1024,512]{1,0:T(8,128)(2,1)}, u32[]{:S(2)}, u32[]{:S(2)}) collective-permute-start(bf16[1024,512]{1,0:T(8,128)(2,1)} %collective-permute-done.1), channel_id=1, source_target_pairs={{0,4},{4,8},{8,12},{12,0},{1,5},{5,9},{9,13},{13,1},{2,6},{6,10},{... | collective-permute-start | bytes 3145736 | tf_op jit(solution)/shard_map/ppermute | solution.py:32
  172.2 0.8 copy-start.3
  172.2 1.0 copy-start.4
  310.3 3.0 copy-start.1
  338.7 44.8 %copy-start = (bf16[256,2048]{1,0:T(8,128)(2,1)S(1)}, bf16[256,2048]{1,0:T(8,128)(2,1)}, u32[]{:S(2)}) copy-start(bf16[256,2048]{1,0:T(8,128)(2,1)} %param.12) | copy-start | bytes 3145732
  338.7 165.2 %all-gather.21.cloned.1.call-start = ((), (), s32[]{:S(2)}) async-start(), calls=%async_computation.9 | async-start | bytes 3932160 | tf_op jit(solution)/shard_map/all_gather | solution.py:146
  339.4 49.5 %copy-start.6 = (bf16[768,512]{1,0:T(8,128)(2,1)S(1)}, bf16[768,512]{1,0:T(8,128)(2,1)}, u32[]{:S(2)}) copy-start(bf16[768,512]{1,0:T(8,128)(2,1)} %param.21) | copy-start | bytes 2359300
  339.4 171.9 %all-gather.19.cloned.1.call-start = ((), (), s32[]{:S(2)}) async-start(), calls=%async_computation.8 | async-start | bytes 5242880 | tf_op jit(solution)/shard_map/all_gather | solution.py:20
  388.1 188.3 %all-gather.23.cloned.1.call-start = ((), (), s32[]{:S(2)}) async-start(), calls=%async_computation.10 | async-start | bytes 3932160 | tf_op jit(solution)/shard_map/all_gather | solution.py:147
  388.9 244.1 %reduce-scatter.5.cloned.1.call-start = ((), (), s32[]{:S(2)}) async-start(), calls=%async_computation.11 | async-start | bytes 5242880 | tf_op jit(solution)/shard_map/reduce_scatter | solution.py:36
  388.9 36.6 %collective-permute-start.3 = (bf16[768,512]{1,0:T(8,128)(2,1)S(1)}, bf16[768,512]{1,0:T(8,128)(2,1)S(1)}, u32[]{:S(2)}, u32[]{:S(2)}) collective-permute-start(bf16[768,512]{1,0:T(8,128)(2,1)S(1)} %copy-done.6), channel_id=1, source_target_pairs={{0,4},{4,8},{8,12},{12,0},{1,5},{5,9},{9,13},{13,1},{2,6},{6,10},{... | collective-permute-start | bytes 2359304 | tf_op jit(solution)/shard_map/ppermute | solution.py:32
  425.5 52.1 %collective-permute-start.4 = (bf16[768,512]{1,0:T(8,128)(2,1)S(1)}, bf16[768,512]{1,0:T(8,128)(2,1)S(1)}, u32[]{:S(2)}, u32[]{:S(2)}) collective-permute-start(bf16[768,512]{1,0:T(8,128)(2,1)S(1)} %collective-permute-done.3), channel_id=1, source_target_pairs={{0,4},{4,8},{8,12},{12,0},{1,5},{5,9},{9,13},{13,1},{2,6},{6,10},{... | collective-permute-start | bytes 2359304 | tf_op jit(solution)/shard_map/ppermute | solution.py:32
  477.6 18.0 %collective-permute-start.5 = (bf16[768,512]{1,0:T(8,128)(2,1)S(1)}, bf16[768,512]{1,0:T(8,128)(2,1)S(1)}, u32[]{:S(2)}, u32[]{:S(2)}) collective-permute-start(bf16[768,512]{1,0:T(8,128)(2,1)S(1)} %collective-permute-done.4), channel_id=1, source_target_pairs={{0,4},{4,8},{8,12},{12,0},{1,5},{5,9},{9,13},{13,1},{2,6},{6,10},{... | collective-permute-start | bytes 2359304 | tf_op jit(solution)/shard_map/ppermute | solution.py:32
  589.6 44.9 %copy-start.2 = (bf16[256,2048]{1,0:T(8,128)(2,1)S(1)}, bf16[256,2048]{1,0:T(8,128)(2,1)}, u32[]{:S(2)}) copy-start(bf16[256,2048]{1,0:T(8,128)(2,1)} %reduce-scatter.3.cloned.1.call-done) | copy-start | bytes 3145732
Sparse Core Ops, SparseCore 0:
  8.9 67.2 all-gather.14
  77.8 32.7 all-gather.8
  112.1 47.6 all-gather.16
  161.2 79.2 all-gather.12
  241.9 79.2 all-gather.10
  338.8 43.0 reduce-scatter.2
  383.5 94.5 all-gather.20
  479.6 31.7 all-gather.18
  513.0 63.4 all-gather.22
  589.7 43.2 reduce-scatter.4
